TPU v7x, 32 devices: a whole 2x2x4 slice. The times are simulated.
32 devices in a mesh: sp: 8 (over z, x), tp: 4 (over y, core).
Axes of the slice: x: 2, y: 2, z: 4, core: 2. Of those that a mesh axis runs over, the one named last changes fastest.
Arguments:
- hidden_states: bfloat16 [6144, 4096], P('sp'), may hold values from -60 to 60
- w_conv_b: bfloat16 [4096, 2048], P(None, 'tp'), may hold values from -0.09375 to 0.09375
- w_conv_c: bfloat16 [4096, 2048], P(None, 'tp'), may hold values from -0.09375 to 0.09375
- w_conv_h: bfloat16 [4096, 2048], P(None, 'tp'), may hold values from -0.09375 to 0.09375
- conv_taps: bfloat16 [3, 2048], P(None, 'tp'), may hold values from -3.5 to 3.5
- w_query: bfloat16 [4096, 2048], P(None, 'tp'), may hold values from -0.15625 to 0.15625
- w_key: bfloat16 [4096, 2048], P(None, 'tp'), may hold values from -0.09375 to 0.09375
- w_value: bfloat16 [4096, 2048], P(None, 'tp'), may hold values from -0.09375 to 0.09375
- lambdas: float32 [16], P('tp'), may hold values from 0.3 to 0.8
- head_gain: bfloat16 [128], replicated, may hold values from 0.099609375 to 1.8984375
- w_out_conv: bfloat16 [2048, 4096], P('tp'), may hold values from -1 to 1
- w_out_attn: bfloat16 [2048, 4096], P('tp'), may hold values from -1 to 1
- out_gain: bfloat16 [4096], replicated, may hold values from 0.099609375 to 1.8984375
Outputs:
- mixed: bfloat16 [6144, 4096], P('sp', 'tp')
All inputs are finite; a program needn't handle non-finite values.
Results may differ from a plain program's by a relative error of at most 0.023.
Values may be sent and summed in bfloat16 or wider, within the bound.
A program may use at most 192 MiB of HBM per device.

v0:
```python
import functools
import math

import jax
import jax.numpy as jnp
import numpy as np
from jax import lax
from jax.experimental import pallas as pl
from jax.experimental.pallas import tpu as pltpu
from jax.sharding import PartitionSpec as P

QK = 64
VD = 128
TILE = 256
SPAN = 256
HEAD_ROWS = 16
NEG_LARGE = -1e30
VMEM_LIMIT = 67_000_000
MESH = pl.DeviceIdType.MESH
BF16, F32 = jnp.bfloat16, jnp.float32


def mixer_kernel(
    n,
    tp,
    turn_ref,
    base_ref,
    taps_ref,
    lam_ref,
    gain_ref,
    out_gain_ref,
    x_hbm,
    wq_ref,
    wk_ref,
    wv_ref,
    wb_ref,
    wc_ref,
    wh_ref,
    w_conv_ref,
    w_attn_ref,
    out_ref,
    x_ref,
    cos_ref,
    sin_ref,
    wbuf,
    q_own,
    kv_own,
    q_all,
    kv_all,
    out_own,
    m_ref,
    l_ref,
    acc_ref,
    lam_all,
    rim_own,
    rim_in,
    first_g,
    first_b,
    conv_chip,
    wc_all,
    wa_all,
    part_out,
    part_in,
    attn_all,
    total_ref,
    stats,
    x_sem,
    w_sem,
    send_q,
    send_kv,
    recv_q,
    recv_kv,
    send_fwd,
    recv_fwd,
    send_o,
    recv_o,
    small_send,
    small_recv,
    send_wa,
    recv_wa,
    send_wc,
    recv_wc,
    local_wc,
    send_part,
    recv_part,
    send_y,
    recv_y,
    send_s,
    recv_s,
    send_stat,
    recv_stat,
):
    j, t = lax.axis_index("sp"), lax.axis_index("tp")
    c, y = t % 2, t // 2
    ranks = tp // 2
    tok, model = x_ref.shape
    width = model // tp
    heads = q_own.shape[0]
    channels = wc_all.shape[2]
    half = n // 2
    repeat = half // heads
    parts = 2 * repeat
    rows = tok // parts
    per = TILE // VD
    pairs, tiles = heads // per, channels // TILE

    def remote(src, dst, send_sem, recv_sem, device):
        return pltpu.make_async_remote_copy(
            src_ref=src,
            dst_ref=dst,
            send_sem=send_sem,
            recv_sem=recv_sem,
            device_id=device,
            device_id_type=MESH,
        )

    sibling = (j, y * 2 + 1 - c)

    def peer(step):
        return (j, (y + step) % ranks * 2 + c)

    barrier = pltpu.get_barrier_semaphore()
    x_copy = pltpu.make_async_copy(x_hbm, x_ref, x_sem)
    x_copy.start()

    qkv_refs, conv_refs = (wq_ref, wk_ref, wv_ref), (wb_ref, wc_ref, wh_ref)

    def load(refs, index, slot):
        for w, ref in enumerate(refs):
            pltpu.make_async_copy(
                ref.at[:, pl.ds(pl.multiple_of(index * TILE, TILE), TILE)],
                wbuf.at[slot, w],
                w_sem.at[slot, w],
            ).start()

    def loaded(refs, slot, w):
        pltpu.make_async_copy(
            refs[w].at[:, pl.ds(0, TILE)], wbuf.at[slot, w], w_sem.at[slot, w]
        ).wait()

    def pair_of(g):
        return (g + j) % pairs

    load(qkv_refs, pair_of(0), 0)

    @pl.loop(0, n)
    def _(a):
        for e in range(2):

            @pl.when(jnp.logical_or(a != j, c != e))
            def _():
                pl.semaphore_signal(
                    barrier, inc=1, device_id=(a, y * 2 + e), device_id_type=MESH
                )

    @pl.loop(1, ranks)
    def _(step):
        for e in range(2):
            pl.semaphore_signal(
                barrier,
                inc=1,
                device_id=(j, (y + step) % ranks * 2 + e),
                device_id_type=MESH,
            )

    lane_row = lax.broadcasted_iota(jnp.int32, (1, VD), 1)
    cos_far, sin_far = base_ref[0, pl.ds(j, 1)], base_ref[1, pl.ds(j, 1)]
    cos_ref[...] = cos_far * turn_ref[0] - sin_far * turn_ref[1]
    sin_ref[...] = jnp.where(lane_row % QK < QK // 2, -1.0, 1.0) * (
        sin_far * turn_ref[0] + cos_far * turn_ref[1]
    )
    for h in range(heads):
        lam_all[c, h : h + 1] = jnp.full((1, VD), lam_ref[h], F32)

    pl.semaphore_wait(barrier, 2 * n - 1 + 2 * (ranks - 1))

    lam_copy = remote(lam_all.at[c], lam_all.at[c], small_send.at[0], small_recv.at[0], sibling)
    lam_copy.start()

    def wa_rows(head, source):
        return wa_all.at[pl.ds(pl.multiple_of((head * tp + source) * VD, VD), VD)]

    def wa_copy(head, target, source):
        return remote(
            w_attn_ref.at[
                pl.ds(head * VD, VD), pl.ds(pl.multiple_of(target * width, VD), width)
            ],
            wa_rows(head, source),
            send_wa.at[target, head],
            recv_wa.at[source, head],
            (j, target),
        )

    def wc_cols(rank, core):
        return w_conv_ref.at[:, pl.ds(pl.multiple_of((rank * 2 + core) * width, VD), width)]

    for head in range(heads):
        pltpu.make_async_copy(
            w_attn_ref.at[pl.ds(head * VD, VD), pl.ds(pl.multiple_of(t * width, VD), width)],
            wa_rows(head, t),
            recv_wa.at[t, head],
        ).start()

    @pl.loop(1, tp)
    def _(step):
        for head in range(heads):
            wa_copy(head, (t + step) % tp, t).start()

    @pl.loop(0, ranks)
    def _(rank):
        pltpu.make_async_copy(wc_cols(rank, c), wc_all.at[rank, c], local_wc.at[rank]).start()
        remote(
            wc_cols(rank, 1 - c), wc_all.at[rank, c], send_wc.at[rank], recv_wc.at[rank], sibling
        ).start()

    def part_of(block, rep, core):
        part = rep * 2 + core
        return jnp.where(block % 2 == 0, part, parts - 1 - part)

    def put(src, dst, send_sem, recv_sem, device, here):
        @pl.when(here)
        def _():
            pltpu.make_async_copy(src, dst, recv_sem).start()

        @pl.when(jnp.logical_not(here))
        def _():
            remote(src, dst, send_sem, recv_sem, device).start()

    def sent(src, send_sem):
        remote(src, src, send_sem, send_sem, sibling).wait_send()

    def put_done(src, send_sem, here):
        @pl.when(jnp.logical_not(here))
        def _():
            sent(src, send_sem)

    def arrived(dst, recv_sem):
        pltpu.make_async_copy(dst, dst, recv_sem).wait()

    lane = lax.broadcasted_iota(jnp.int32, (tok, VD), 1)
    low = lane % QK < QK // 2
    fold = QK ** (-0.5) * math.log2(math.e)

    def rotate(values):
        values = values.astype(F32)
        partner = jnp.where(
            low, pltpu.roll(values, VD - QK // 2, 1), pltpu.roll(values, QK // 2, 1)
        )
        return values * cos_ref[...] + partner * sin_ref[...]

    def project(slot, w):
        return jnp.dot(x_ref[...], wbuf[slot, w], preferred_element_type=F32).astype(BF16)

    x_copy.wait()

    @pl.loop(0, pairs)
    def _(g):
        slot = g % 2

        @pl.when(g + 1 < pairs)
        def _():
            load(qkv_refs, pair_of(g + 1), 1 - slot)

        @pl.when(g + 1 == pairs)
        def _():
            load(conv_refs, 0, 1 - slot)

        pair = pair_of(g)

        def send_kv_of(e):
            for p in range(per):
                head = pair * per + p
                for r in range(repeat):
                    local = head * repeat + r
                    s = c * half + local
                    put(
                        kv_own.at[e, head],
                        kv_all.at[e, j],
                        send_kv.at[local * 2 + e],
                        recv_kv.at[j],
                        (s, y * 2 + e),
                        jnp.logical_and(s == j, c == e),
                    )

        loaded(qkv_refs, slot, 1)
        k = project(slot, 1)
        for p in range(per):
            kv_own[0, pair * per + p] = rotate(k[:, p * VD : (p + 1) * VD]).astype(BF16)
        loaded(qkv_refs, slot, 2)
        send_kv_of(0)
        v = project(slot, 2)
        for p in range(per):
            kv_own[1, pair * per + p] = v[:, p * VD : (p + 1) * VD]
        loaded(qkv_refs, slot, 0)
        send_kv_of(1)
        q = project(slot, 0)
        for p in range(per):
            q_own[pair * per + p] = (rotate(q[:, p * VD : (p + 1) * VD]) * fold).astype(BF16)
        for p in range(per):
            head = pair * per + p
            for r in range(repeat):
                local = head * repeat + r
                s = c * half + local
                for e in range(2):
                    first = pl.multiple_of(part_of(j, r, e) * rows, 16)
                    put(
                        q_own.at[head, pl.ds(first, rows)],
                        q_all.at[j],
                        send_q.at[local * 2 + e],
                        recv_q.at[j],
                        (s, y * 2 + e),
                        jnp.logical_and(s == j, c == e),
                    )

    @pl.loop(0, tiles)
    def _(g):
        slot = (pairs + g) % 2

        @pl.when(g + 1 < tiles)
        def _():
            load(conv_refs, g + 1, 1 - slot)

        for w in range(3):
            loaded(conv_refs, slot, w)
        cols = pl.ds(pl.multiple_of(g * TILE, TILE), TILE)
        gated = project(slot, 1).astype(F32) * project(slot, 2).astype(F32)
        row = lax.broadcasted_iota(jnp.int32, gated.shape, 0)
        back_one = jnp.where(row == 0, 0.0, pltpu.roll(gated, 1, 0))
        back_two = jnp.where(row < 2, 0.0, pltpu.roll(gated, 2, 0))
        tap = taps_ref[:, cols].astype(F32)
        conv = tap[0:1] * back_two + tap[1:2] * back_one + tap[2:3] * gated
        gate = project(slot, 0).astype(F32)
        conv_chip[c, :, cols] = (gate * conv).astype(BF16)
        first_g[:, cols] = gated[:HEAD_ROWS]
        first_b[:, cols] = gate[:HEAD_ROWS]
        rim_own[:, cols] = gated[tok - 8 :]

    rim_copy = remote(
        rim_own, rim_in, small_send.at[1], small_recv.at[1], (jnp.minimum(j + 1, n - 1), t)
    )

    @pl.when(j + 1 < n)
    def _():
        rim_copy.start()

    lam_copy.wait()

    side = j // half
    head_at = (j % half) // repeat
    rep_at = j % repeat
    owner_tp = y * 2 + side
    lam = lam_all[side, pl.ds(head_at, 1)]
    gain = gain_ref[...].astype(F32)
    block_lane = lax.broadcasted_iota(jnp.int32, (rows, VD), 1)

    def forward(block):
        here = kv_all.at[c, block]
        arrived(here, recv_kv.at[block])
        remote(here, here, send_fwd.at[block], recv_fwd.at[block], sibling).start()

    def attend(slot, kb, both, part, masked):
        k, v = kv_all[0, kb], kv_all[1, kb]
        s = lax.dot_general(both, k, (((1,), (1,)), ((), ())), preferred_element_type=F32)
        if masked:
            r = part * rows + lax.broadcasted_iota(jnp.int32, s.shape, 0) % rows
            s = jnp.where(lax.broadcasted_iota(jnp.int32, s.shape, 1) <= r, s, NEG_LARGE)
        slabs = [s[:, b * VD : (b + 1) * VD] for b in range(tok // VD)]
        old = m_ref[slot]
        top = functools.reduce(jnp.maximum, slabs)
        new = jnp.maximum(old, jnp.max(top, axis=1, keepdims=True))
        factor = jnp.exp2(old - new)
        total = l_ref[slot] * factor
        weights = []
        for slab in slabs:
            w = jnp.exp2(slab - new)
            total = total + w
            weights.append(w.astype(BF16))
        m_ref[slot] = new
        l_ref[slot] = total
        acc_ref[slot] = acc_ref[slot] * factor + jnp.dot(
            jnp.concatenate(weights, axis=1), v, preferred_element_type=F32
        )

    def piece(head, source, part):
        return attn_all.at[
            pl.ds(pl.multiple_of(part * rows, 16), rows),
            pl.ds(pl.multiple_of((head * tp + source) * VD, VD), VD),
        ]

    def piece_of(k, core, source):
        local = (j - k) % half
        head, rep = local // repeat, local % repeat
        return local * 2 + core, piece(head, source, part_of(j, rep, core))

    def share(k):
        for core in range(2):
            index, mine = piece_of(k, core, t)
            arrived(mine, recv_o.at[index])

            @pl.loop(1, ranks)
            def _(step):
                remote(
                    mine, mine, send_y.at[step, index], recv_y.at[step, index], peer(step)
                ).start()

            remote(mine, mine, send_s.at[y, index], recv_s.at[y, index], sibling).start()

    def relay(k):
        @pl.loop(1, ranks)
        def _(step):
            rank = (y + ranks - step) % ranks
            for core in range(2):
                index, theirs = piece_of(k, core, rank * 2 + c)
                arrived(theirs, recv_y.at[step, index])
                remote(
                    theirs, theirs, send_s.at[rank, index], recv_s.at[rank, index], sibling
                ).start()

    def gathered(k):
        @pl.loop(0, ranks)
        def _(rank):
            for core in range(2):
                index, theirs = piece_of(k, core, rank * 2 + 1 - c)
                arrived(theirs, recv_s.at[rank, index])

    def fix_first_rows():
        @pl.when(j > 0)
        def _():
            rim_copy.wait_recv()

        taps = taps_ref[...].astype(F32)
        before = jnp.where(j > 0, rim_in[...], 0.0)
        gated, gate = first_g[...], first_b[...]
        row = lax.broadcasted_iota(jnp.int32, gated.shape, 0)
        one, two = before[7:8], before[6:7]
        back_one = jnp.where(row == 0, one, pltpu.roll(gated, 1, 0))
        back_two = jnp.where(row == 0, two, jnp.where(row == 1, one, pltpu.roll(gated, 2, 0)))
        conv = taps[0:1] * back_two + taps[1:2] * back_one + taps[2:3] * gated
        conv_chip[c, :HEAD_ROWS] = (gate * conv).astype(BF16)

    conv_copy = remote(
        conv_chip.at[c], conv_chip.at[c], small_send.at[2], small_recv.at[2], sibling
    )

    def conv_product(first, rank):
        span = pl.ds(first, SPAN)
        return jnp.dot(
            conv_chip[0, span], wc_all[rank, 0], preferred_element_type=F32
        ) + jnp.dot(conv_chip[1, span], wc_all[rank, 1], preferred_element_type=F32)

    def conv_parts():
        conv_copy.wait_recv()

        @pl.loop(0, ranks)
        def _(rank):
            mine = wc_all.at[rank, c]
            theirs = wc_all.at[rank, 1 - c]
            arrived(mine, local_wc.at[rank])
            arrived(theirs, recv_wc.at[rank])

        @pl.loop(1, ranks)
        def _(step):
            @pl.loop(0, tok // SPAN)
            def _(b):
                first = pl.multiple_of(b * SPAN, SPAN)
                part_out[step - 1, pl.ds(first, SPAN)] = conv_product(
                    first, (y + step) % ranks
                ).astype(BF16)

            remote(
                part_out.at[step - 1],
                part_in.at[step - 1],
                send_part.at[step - 1],
                recv_part.at[step - 1],
                peer(step),
            ).start()

    @pl.loop(0, 3 * half)
    def _(step):
        phase = step // half
        turn = (step + j) % half
        group = jnp.where(phase == 0, side, jnp.where(phase == 1, 1 - side, 1))
        block = group * half + turn
        base = group * half
        slot = jnp.where(group == 0, half, turn)

        @pl.when(jnp.logical_and(step % half == 0, phase < 2))
        def _():
            @pl.loop(0, half)
            def _(b):
                forward(base + b)

            @pl.loop(0, half)
            def _(b):
                arrived(q_all.at[base + b], recv_q.at[base + b])
                arrived(kv_all.at[1 - c, base + b], recv_fwd.at[base + b])

        @pl.when(step == 1)
        def _():
            fix_first_rows()
            conv_copy.start()

        @pl.when(step == 2)
        def _():
            conv_parts()

        @pl.when(step > 2 * half)
        def _():
            share(step - 2 * half - 1)

        @pl.when(step > 2 * half + 1)
        def _():
            relay(step - 2 * half - 2)

        q = q_all[block]
        zero = jnp.zeros_like(q)
        both = jnp.concatenate(
            [jnp.where(block_lane < QK, q, zero), jnp.where(block_lane < QK, zero, q)], axis=0
        )
        part = part_of(block, rep_at, c)

        @pl.when(phase < 2)
        def _():
            m_ref[slot] = jnp.full(m_ref.shape[1:], NEG_LARGE, F32)
            l_ref[slot] = jnp.zeros(l_ref.shape[1:], F32)
            acc_ref[slot] = jnp.zeros(acc_ref.shape[1:], F32)

        @pl.loop(jnp.where(phase == 2, 0, base), jnp.where(phase == 2, half, block))
        def _(kb):
            attend(slot, kb, both, part, False)

        @pl.when(phase < 2)
        def _():
            attend(slot, block, both, part, True)

        @pl.when(jnp.logical_or(phase == 2, group == 0))
        def _():
            first, second = (
                acc_ref[slot, span] / jnp.sum(l_ref[slot, span], axis=1, keepdims=True)
                for span in (pl.ds(0, rows), pl.ds(rows, rows))
            )
            diff = first - lam * second
            norm = lax.rsqrt(jnp.mean(diff * diff, axis=1, keepdims=True) + 1e-05)
            out_own[block] = (diff * norm * gain).astype(BF16)
            put(
                out_own.at[block],
                piece(head_at, owner_tp, part),
                send_o.at[block],
                recv_o.at[(j % half) * 2 + c],
                (block, owner_tp),
                jnp.logical_and(block == j, side == c),
            )

    share(half - 1)
    relay(half - 2)

    @pl.loop(1, ranks)
    def _(step):
        arrived(part_in.at[step - 1], recv_part.at[step - 1])

    @pl.loop(0, tok // SPAN)
    def _(b):
        first = pl.multiple_of(b * SPAN, SPAN)
        value = conv_product(first, y)
        for step in range(1, ranks):
            value = value + part_in[step - 1, pl.ds(first, SPAN)].astype(F32)
        total_ref[pl.ds(first, SPAN)] = value

    @pl.loop(0, tp)
    def _(source):
        for head in range(heads):
            arrived(wa_rows(head, source), recv_wa.at[source, head])

    def accumulate(k):
        gathered(k)
        local = (j - k) % half
        head, rep = local // repeat, local % repeat
        deep = pl.ds(pl.multiple_of(head * tp * VD, VD), tp * VD)
        for core in range(2):
            span = pl.ds(pl.multiple_of(part_of(j, rep, core) * rows, 16), rows)
            total_ref[span] = total_ref[span] + jnp.dot(
                attn_all[span, deep], wa_all[deep], preferred_element_type=F32
            )

    @pl.loop(0, half)
    def _(k):
        @pl.when(k == half - 1)
        def _():
            relay(half - 1)

        accumulate(k)

    slabs = width // VD

    @pl.loop(0, tok // SPAN)
    def _(b):
        span = pl.ds(pl.multiple_of(b * SPAN, SPAN), SPAN)
        mix = total_ref[span].astype(BF16)
        out_ref[span] = mix
        sums = jnp.zeros((SPAN, VD), F32)
        squares = jnp.zeros((SPAN, VD), F32)
        for s in range(slabs):
            slab = mix[:, s * VD : (s + 1) * VD].astype(F32)
            sums = sums + slab
            squares = squares + slab * slab
        stats[t, 0:1, span] = jnp.sum(sums.T, axis=0, keepdims=True)
        stats[t, 1:2, span] = jnp.sum(squares.T, axis=0, keepdims=True)

    def stat_copy(step):
        return remote(
            stats.at[t],
            stats.at[t],
            send_stat.at[step],
            recv_stat.at[step],
            (j, (t + step) % tp),
        )

    @pl.loop(1, tp)
    def _(step):
        stat_copy(step).start()

    own_gain = out_gain_ref[:, pl.ds(pl.multiple_of(t * width, VD), width)].astype(F32)

    @pl.loop(1, tp)
    def _(step):
        source = (t + tp - step) % tp
        arrived(stats.at[source], recv_stat.at[step])

    @pl.loop(0, tok // SPAN)
    def _(b):
        span = pl.ds(pl.multiple_of(b * SPAN, SPAN), SPAN)
        sums, squares = stats[0, 0:1, span], stats[0, 1:2, span]
        for source in range(1, tp):
            sums = sums + stats[source, 0:1, span]
            squares = squares + stats[source, 1:2, span]
        mean = sums / model
        scale = lax.rsqrt(squares / model - mean * mean + 1e-05)
        mean_cols = jnp.broadcast_to(mean, (VD, SPAN)).T
        scale_cols = jnp.broadcast_to(scale, (VD, SPAN)).T
        for s in range(slabs):
            cols = slice(s * VD, (s + 1) * VD)
            value = (out_ref[span, cols].astype(F32) - mean_cols) * scale_cols
            out_ref[span, cols] = (value * own_gain[:, cols]).astype(BF16)


    @pl.when(j + 1 < n)
    def _():
        rim_copy.wait_send()

    conv_copy.wait_send()

    @pl.loop(0, half)
    def _(local):
        head = local // repeat
        s = c * half + local
        for e in range(2):
            here = jnp.logical_and(s == j, c == e)
            put_done(kv_own.at[e, head], send_kv.at[local * 2 + e], here)
            put_done(q_own.at[head, pl.ds(0, rows)], send_q.at[local * 2 + e], here)

    @pl.loop(0, n)
    def _(block):
        sent(kv_all.at[c, block], send_fwd.at[block])
        put_done(out_own.at[block], send_o.at[block], jnp.logical_and(block == j, side == c))

        @pl.loop(1, ranks)
        def _(step):
            sent(out_own.at[0], send_y.at[step, block])

        @pl.loop(0, ranks)
        def _(rank):
            sent(out_own.at[0], send_s.at[rank, block])

    @pl.loop(1, tp)
    def _(step):
        stat_copy(step).wait_send()
        for head in range(heads):
            sent(wa_rows(head, t), send_wa.at[(t + step) % tp, head])

    @pl.loop(0, ranks)
    def _(rank):
        sent(wc_all.at[rank, c], send_wc.at[rank])

    @pl.loop(1, ranks)
    def _(step):
        sent(part_out.at[step - 1], send_part.at[step - 1])


def per_device(
    n,
    tp,
    hidden_states,
    w_conv_b,
    w_conv_c,
    w_conv_h,
    conv_taps,
    w_query,
    w_key,
    w_value,
    lambdas,
    head_gain,
    w_out_conv,
    w_out_attn,
    out_gain,
):
    tok, model = hidden_states.shape
    heads = w_value.shape[1] // VD
    channels = w_conv_b.shape[1]
    half = n // 2
    repeat = half // heads
    parts = 2 * repeat
    rows = tok // parts
    ranks = tp // 2
    width = model // tp

    inverse = 10000.0 ** (-np.arange(0, QK, 2, dtype=np.float64) / QK)
    inverse = np.tile(inverse, VD // inverse.size)[None, :]
    table = lambda angles: np.stack([np.cos(angles), np.sin(angles)]).astype(np.float32)
    turn = table(np.arange(tok)[:, None] * inverse)
    base = table(np.arange(n)[:, None] * tok * inverse)
    lam_rows = -(-heads // 8) * 8

    vmem, hbm = pl.BlockSpec(memory_space=pltpu.VMEM), pl.BlockSpec(memory_space=pl.ANY)
    smem = pl.BlockSpec(memory_space=pltpu.SMEM)
    dma = pltpu.SemaphoreType.DMA
    return pl.pallas_call(
        functools.partial(mixer_kernel, n, tp),
        out_shape=jax.ShapeDtypeStruct((tok, width), BF16),
        in_specs=[vmem] * 3 + [smem] + [vmem] * 2 + [hbm] * 9,
        out_specs=vmem,
        scratch_shapes=[
            pltpu.VMEM((tok, model), BF16),
            pltpu.VMEM((tok, VD), F32),
            pltpu.VMEM((tok, VD), F32),
            pltpu.VMEM((2, 3, model, TILE), BF16),
            pltpu.VMEM((heads, tok, VD), BF16),
            pltpu.VMEM((2, heads, tok, VD), BF16),
            pltpu.VMEM((n, rows, VD), BF16),
            pltpu.VMEM((2, n, tok, VD), BF16),
            pltpu.VMEM((n, rows, VD), BF16),
            pltpu.VMEM((half + 1, 2 * rows, VD), F32),
            pltpu.VMEM((half + 1, 2 * rows, VD), F32),
            pltpu.VMEM((half + 1, 2 * rows, VD), F32),
            pltpu.VMEM((2, lam_rows, VD), F32),
            pltpu.VMEM((8, channels), F32),
            pltpu.VMEM((8, channels), F32),
            pltpu.VMEM((HEAD_ROWS, channels), F32),
            pltpu.VMEM((HEAD_ROWS, channels), F32),
            pltpu.VMEM((2, tok, channels), BF16),
            pltpu.VMEM((ranks, 2, channels, width), BF16),
            pltpu.VMEM((heads * tp * VD, width), BF16),
            pltpu.VMEM((max(ranks - 1, 1), tok, width), BF16),
            pltpu.VMEM((max(ranks - 1, 1), tok, width), BF16),
            pltpu.VMEM((tok, heads * tp * VD), BF16),
            pltpu.VMEM((tok, width), F32),
            pltpu.VMEM((tp, 8, tok), F32),
            dma,
            dma((2, 3)),
            dma((n,)),
            dma((n,)),
            dma((n,)),
            dma((n,)),
            dma((n,)),
            dma((n,)),
            dma((n,)),
            dma((n,)),
            dma((3,)),
            dma((3,)),
            dma((tp, heads)),
            dma((tp, heads)),
            dma((ranks,)),
            dma((ranks,)),
            dma((ranks,)),
            dma((ranks,)),
            dma((ranks,)),
            dma((ranks, n)),
            dma((ranks, n)),
            dma((ranks, n)),
            dma((ranks, n)),
            dma((tp,)),
            dma((tp,)),
        ],
        compiler_params=pltpu.CompilerParams(
            vmem_limit_bytes=VMEM_LIMIT, collective_id=0, has_side_effects=True
        ),
        cost_estimate=pl.CostEstimate(
            flops=12 * tok * model * channels + 4 * n * n * rows * tok * VD,
            bytes_accessed=2 * model * (tok + 6 * channels),
            transcendentals=0,
        ),
        name="mixer",
    )(
        jnp.asarray(turn),
        jnp.asarray(base),
        conv_taps,
        lambdas,
        head_gain[None],
        out_gain[None],
        hidden_states,
        w_query,
        w_key,
        w_value,
        w_conv_b,
        w_conv_c,
        w_conv_h,
        w_out_conv,
        w_out_attn,
    )


def solution(mesh):
    n, tp = mesh.shape["sp"], mesh.shape["tp"]
    return jax.shard_map(
        functools.partial(per_device, n, tp),
        mesh=mesh,
        in_specs=(
            P("sp", None),
            P(None, "tp"),
            P(None, "tp"),
            P(None, "tp"),
            P(None, "tp"),
            P(None, "tp"),
            P(None, "tp"),
            P(None, "tp"),
            P("tp"),
            P(),
            P("tp", None),
            P("tp", None),
            P(),
        ),
        out_specs=P("sp", "tp"),
        check_vma=False,
    )
```

profile of v0, /device:TPU:23, one launch (start us, length us, event | category | flops | bytes accessed | tf_op | source)
XLA Modules:
  0.0 140.3 jit_solution(12922982682950633180)
XLA Ops:
  0.0 1.3 broadcast_in_dim.7.out_gain_ref
  1.3 136.3 %mixer.1 = bf16[768,1024]{1,0:T(8,128)(2,1)} custom-call(f32[2,768,128]{2,1,0:T(8,128)} %constant.4.clone.turn_ref, f32[2,8,128]{2,1,0:T(8,128)} %constant.5.clone.base_ref, bf16[3,512]{1,0:T(4,128)(2,1)} %taps_ref.1, f32[4]{0:T(128)} %lam_ref.1, bf16[1,128]{1,0:T(2,128)(2,1)} %bitcast.1, bf16[1,4096]{1,0:T(2,128)(2,1)} %broadcast_in_dim.7.out_gain_ref, ...), custom_call_target="tpu_custom_call" | custom-call | flops 28991029248 | bytes 31457280 | tf_op jit(solution)/shard_map/mixer/pallas_call | solution.py:726
  137.7 2.7 %copy.17 = bf16[768,1024]{1,0:T(8,128)(2,1)} copy(bf16[768,1024]{1,0:T(8,128)(2,1)} %mixer.1) | data formatting | bytes 3145728
where the time goes:
time: 141 us; the launch traced here: 140 us
  Pallas kernels  136 us (96%)
  local copies, waits for them, and re-layouts  3.98 us (3%)
    pallas_call x1, Pallas kernels, per_device(): pl.pallas_call(functools.partial(mixer_kernel, n, tp), out_shape=jax.Shap...  136 us

commit v1 on v0

--- a/solution.py
+++ b/solution.py
@@ -13,7 +13,8 @@
 VD = 128
 TILE = 256
 SPAN = 256
-HEAD_ROWS = 16
+RIM = 16
+RING = 4
 NEG_LARGE = -1e30
 VMEM_LIMIT = 67_000_000
 MESH = pl.DeviceIdType.MESH
@@ -28,7 +29,6 @@
     taps_ref,
     lam_ref,
     gain_ref,
-    out_gain_ref,
     x_hbm,
     wq_ref,
     wk_ref,
@@ -39,10 +39,13 @@
     w_conv_ref,
     w_attn_ref,
     out_ref,
+    stat_ref,
     x_ref,
     cos_ref,
     sin_ref,
+    tables,
     wbuf,
+    raw_ref,
     q_own,
     kv_own,
     q_all,
@@ -52,10 +55,8 @@
     l_ref,
     acc_ref,
     lam_all,
-    rim_own,
-    rim_in,
-    first_g,
-    first_b,
+    rim_x,
+    rim_raw,
     conv_chip,
     wc_all,
     wa_all,
@@ -65,6 +66,7 @@
     total_ref,
     stats,
     x_sem,
+    turn_sem,
     w_sem,
     send_q,
     send_kv,
@@ -78,6 +80,7 @@
     small_recv,
     send_wa,
     recv_wa,
+    send_wf,
     send_wc,
     recv_wc,
     local_wc,
@@ -123,25 +126,35 @@
     x_copy = pltpu.make_async_copy(x_hbm, x_ref, x_sem)
     x_copy.start()
 
-    qkv_refs, conv_refs = (wq_ref, wk_ref, wv_ref), (wb_ref, wc_ref, wh_ref)
-
-    def load(refs, index, slot):
-        for w, ref in enumerate(refs):
-            pltpu.make_async_copy(
-                ref.at[:, pl.ds(pl.multiple_of(index * TILE, TILE), TILE)],
-                wbuf.at[slot, w],
-                w_sem.at[slot, w],
-            ).start()
-
-    def loaded(refs, slot, w):
-        pltpu.make_async_copy(
-            refs[w].at[:, pl.ds(0, TILE)], wbuf.at[slot, w], w_sem.at[slot, w]
-        ).wait()
-
-    def pair_of(g):
-        return (g + j) % pairs
-
-    load(qkv_refs, pair_of(0), 0)
+    turn_copy = pltpu.make_async_copy(turn_ref, tables, turn_sem)
+    turn_copy.start()
+    products = 3 * (pairs + tiles)
+    side = j // half
+    early = c == side
+    shift = jnp.where(jnp.logical_and(side == 1, c == 0), 0, 1)
+    lead = jnp.where(early, 0, 3 * ((tiles + 1) // 2))
+
+    def product(i):
+        is_conv = jnp.logical_or(i < lead, i >= lead + 3 * pairs)
+        r = jnp.where(i < lead, i, i - 3 * pairs)
+        q = i - lead
+        kind = jnp.where(is_conv, 3 + r % 3, (q // pairs + shift) % 3)
+        index = jnp.where(is_conv, r // 3, (q % pairs + j) % pairs)
+        return kind, index
+
+    def load(i):
+        kind, index = product(i)
+        for w, ref in enumerate((wq_ref, wk_ref, wv_ref, wb_ref, wc_ref, wh_ref)):
+
+            @pl.when(kind == w)
+            def _():
+                pltpu.make_async_copy(
+                    ref.at[:, pl.ds(pl.multiple_of(index * TILE, TILE), TILE)],
+                    wbuf.at[i % RING],
+                    w_sem.at[i % RING],
+                ).start()
+
+    load(0)
 
     @pl.loop(0, n)
     def _(a):
@@ -165,53 +178,110 @@
 
     lane_row = lax.broadcasted_iota(jnp.int32, (1, VD), 1)
     cos_far, sin_far = base_ref[0, pl.ds(j, 1)], base_ref[1, pl.ds(j, 1)]
-    cos_ref[...] = cos_far * turn_ref[0] - sin_far * turn_ref[1]
+    turn_copy.wait()
+    cos_ref[...] = cos_far * tables[0] - sin_far * tables[1]
     sin_ref[...] = jnp.where(lane_row % QK < QK // 2, -1.0, 1.0) * (
-        sin_far * turn_ref[0] + cos_far * turn_ref[1]
+        sin_far * tables[0] + cos_far * tables[1]
     )
+    for i in range(1, RING - 1):
+        load(i)
     for h in range(heads):
         lam_all[c, h : h + 1] = jnp.full((1, VD), lam_ref[h], F32)
 
-    pl.semaphore_wait(barrier, 2 * n - 1 + 2 * (ranks - 1))
-
+    rim_copy = remote(
+        x_ref.at[pl.ds(tok - RIM, RIM)],
+        rim_x,
+        small_send.at[1],
+        small_recv.at[1],
+        (jnp.minimum(j + 1, n - 1), t),
+    )
     lam_copy = remote(lam_all.at[c], lam_all.at[c], small_send.at[0], small_recv.at[0], sibling)
-    lam_copy.start()
 
     def wa_rows(head, source):
         return wa_all.at[pl.ds(pl.multiple_of((head * tp + source) * VD, VD), VD)]
 
-    def wa_copy(head, target, source):
-        return remote(
-            w_attn_ref.at[
-                pl.ds(head * VD, VD), pl.ds(pl.multiple_of(target * width, VD), width)
-            ],
-            wa_rows(head, source),
-            send_wa.at[target, head],
-            recv_wa.at[source, head],
-            (j, target),
-        )
+    def wa_block(head, target):
+        return w_attn_ref.at[
+            pl.ds(pl.multiple_of(head * VD, VD), VD),
+            pl.ds(pl.multiple_of(target * width, VD), width),
+        ]
 
     def wc_cols(rank, core):
         return w_conv_ref.at[:, pl.ds(pl.multiple_of((rank * 2 + core) * width, VD), width)]
 
-    for head in range(heads):
-        pltpu.make_async_copy(
-            w_attn_ref.at[pl.ds(head * VD, VD), pl.ds(pl.multiple_of(t * width, VD), width)],
-            wa_rows(head, t),
-            recv_wa.at[t, head],
-        ).start()
-
-    @pl.loop(1, tp)
-    def _(step):
+    near = heads // 2
+    first_near = (j % 2) * near
+
+    def local_weights():
         for head in range(heads):
-            wa_copy(head, (t + step) % tp, t).start()
-
-    @pl.loop(0, ranks)
-    def _(rank):
-        pltpu.make_async_copy(wc_cols(rank, c), wc_all.at[rank, c], local_wc.at[rank]).start()
-        remote(
-            wc_cols(rank, 1 - c), wc_all.at[rank, c], send_wc.at[rank], recv_wc.at[rank], sibling
-        ).start()
+            pltpu.make_async_copy(
+                wa_block(head, t), wa_rows(head, t), recv_wa.at[t, head]
+            ).start()
+
+        @pl.loop(0, ranks)
+        def _(rank):
+            pltpu.make_async_copy(wc_cols(rank, c), wc_all.at[rank, c], local_wc.at[rank]).start()
+
+    def early_sends():
+        pl.semaphore_wait(barrier, 2 * n - 1 + 2 * (ranks - 1))
+
+        @pl.when(j + 1 < n)
+        def _():
+            rim_copy.start()
+
+        lam_copy.start()
+
+        @pl.loop(1, ranks)
+        def _(step):
+            for e in range(2):
+                target = (y + step) % ranks * 2 + e
+                for h in range(near):
+                    head = first_near + h
+                    remote(
+                        wa_block(head, target),
+                        wa_rows(head, t),
+                        send_wa.at[target, head],
+                        recv_wa.at[t, head],
+                        (j, target),
+                    ).start()
+
+    def sibling_weights():
+        for head in range(heads):
+            target = y * 2 + 1 - c
+            remote(
+                wa_block(head, target),
+                wa_rows(head, t),
+                send_wa.at[target, head],
+                recv_wa.at[t, head],
+                sibling,
+            ).start()
+
+        @pl.loop(0, ranks)
+        def _(rank):
+            remote(
+                wc_cols(rank, 1 - c),
+                wc_all.at[rank, c],
+                send_wc.at[rank],
+                recv_wc.at[rank],
+                sibling,
+            ).start()
+
+    def pass_weights():
+        @pl.loop(1, ranks)
+        def _(step):
+            for e in range(2):
+                source = (y + step) % ranks * 2 + e
+                for h in range(near):
+                    head = first_near + h
+                    block = wa_rows(head, source)
+                    arrived(block, recv_wa.at[source, head])
+                    remote(
+                        block,
+                        block,
+                        send_wf.at[source, h],
+                        recv_wa.at[source, head],
+                        (j + 1 - 2 * (j % 2), t),
+                    ).start()
 
     def part_of(block, rep, core):
         part = rep * 2 + core
@@ -248,54 +318,22 @@
         )
         return values * cos_ref[...] + partner * sin_ref[...]
 
-    def project(slot, w):
-        return jnp.dot(x_ref[...], wbuf[slot, w], preferred_element_type=F32).astype(BF16)
-
-    x_copy.wait()
-
-    @pl.loop(0, pairs)
-    def _(g):
-        slot = g % 2
-
-        @pl.when(g + 1 < pairs)
-        def _():
-            load(qkv_refs, pair_of(g + 1), 1 - slot)
-
-        @pl.when(g + 1 == pairs)
-        def _():
-            load(conv_refs, 0, 1 - slot)
-
-        pair = pair_of(g)
-
-        def send_kv_of(e):
-            for p in range(per):
-                head = pair * per + p
-                for r in range(repeat):
-                    local = head * repeat + r
-                    s = c * half + local
-                    put(
-                        kv_own.at[e, head],
-                        kv_all.at[e, j],
-                        send_kv.at[local * 2 + e],
-                        recv_kv.at[j],
-                        (s, y * 2 + e),
-                        jnp.logical_and(s == j, c == e),
-                    )
-
-        loaded(qkv_refs, slot, 1)
-        k = project(slot, 1)
+    def send_kv_of(e, pair):
         for p in range(per):
-            kv_own[0, pair * per + p] = rotate(k[:, p * VD : (p + 1) * VD]).astype(BF16)
-        loaded(qkv_refs, slot, 2)
-        send_kv_of(0)
-        v = project(slot, 2)
-        for p in range(per):
-            kv_own[1, pair * per + p] = v[:, p * VD : (p + 1) * VD]
-        loaded(qkv_refs, slot, 0)
-        send_kv_of(1)
-        q = project(slot, 0)
-        for p in range(per):
-            q_own[pair * per + p] = (rotate(q[:, p * VD : (p + 1) * VD]) * fold).astype(BF16)
+            head = pair * per + p
+            for r in range(repeat):
+                local = head * repeat + r
+                s = c * half + local
+                put(
+                    kv_own.at[e, head],
+                    kv_all.at[e, j],
+                    send_kv.at[local * 2 + e],
+                    recv_kv.at[j],
+                    (s, y * 2 + e),
+                    jnp.logical_and(s == j, c == e),
+                )
+
+    def send_q_of(pair):
         for p in range(per):
             head = pair * per + p
             for r in range(repeat):
@@ -312,51 +350,138 @@
                         jnp.logical_and(s == j, c == e),
                     )
 
-    @pl.loop(0, tiles)
-    def _(g):
-        slot = (pairs + g) % 2
-
-        @pl.when(g + 1 < tiles)
-        def _():
-            load(conv_refs, g + 1, 1 - slot)
-
-        for w in range(3):
-            loaded(conv_refs, slot, w)
+    def convolve(g):
         cols = pl.ds(pl.multiple_of(g * TILE, TILE), TILE)
-        gated = project(slot, 1).astype(F32) * project(slot, 2).astype(F32)
+        gated = raw_ref[1].astype(F32) * raw_ref[2].astype(F32)
+        before = jnp.where(j > 0, rim_raw[0] * rim_raw[1], 0.0)
+        one, two = before[RIM - 1 :], before[RIM - 2 : RIM - 1]
         row = lax.broadcasted_iota(jnp.int32, gated.shape, 0)
-        back_one = jnp.where(row == 0, 0.0, pltpu.roll(gated, 1, 0))
-        back_two = jnp.where(row < 2, 0.0, pltpu.roll(gated, 2, 0))
+        back_one = jnp.where(row == 0, one, pltpu.roll(gated, 1, 0))
+        back_two = jnp.where(row == 0, two, jnp.where(row == 1, one, pltpu.roll(gated, 2, 0)))
         tap = taps_ref[:, cols].astype(F32)
         conv = tap[0:1] * back_two + tap[1:2] * back_one + tap[2:3] * gated
-        gate = project(slot, 0).astype(F32)
-        conv_chip[c, :, cols] = (gate * conv).astype(BF16)
-        first_g[:, cols] = gated[:HEAD_ROWS]
-        first_b[:, cols] = gate[:HEAD_ROWS]
-        rim_own[:, cols] = gated[tok - 8 :]
-
-    rim_copy = remote(
-        rim_own, rim_in, small_send.at[1], small_recv.at[1], (jnp.minimum(j + 1, n - 1), t)
+        conv_chip[c, :, cols] = (raw_ref[0].astype(F32) * conv).astype(BF16)
+
+
+    def forward(block):
+        here = kv_all.at[c, block]
+        arrived(here, recv_kv.at[block])
+        remote(here, here, send_fwd.at[block], recv_fwd.at[block], sibling).start()
+
+    def keys_sent(first):
+        @pl.loop(0, half)
+        def _(b):
+            forward(first + b)
+
+    conv_copy = remote(
+        conv_chip.at[c], conv_chip.at[c], small_send.at[2], small_recv.at[2], sibling
     )
 
-    @pl.when(j + 1 < n)
-    def _():
-        rim_copy.start()
+    def conv_product(first, rank):
+        span = pl.ds(first, SPAN)
+        return jnp.dot(
+            conv_chip[0, span], wc_all[rank, 0], preferred_element_type=F32
+        ) + jnp.dot(conv_chip[1, span], wc_all[rank, 1], preferred_element_type=F32)
+
+    def conv_parts():
+        conv_copy.wait_recv()
+
+        @pl.loop(0, ranks)
+        def _(rank):
+            mine = wc_all.at[rank, c]
+            theirs = wc_all.at[rank, 1 - c]
+            arrived(mine, local_wc.at[rank])
+            arrived(theirs, recv_wc.at[rank])
+
+        @pl.loop(1, ranks)
+        def _(step):
+            @pl.loop(0, tok // SPAN)
+            def _(b):
+                first = pl.multiple_of(b * SPAN, SPAN)
+                span = pl.ds(first, SPAN)
+                part_out[step - 1, span] = conv_product(first, (y + step) % ranks).astype(BF16)
+                remote(
+                    part_out.at[step - 1, span],
+                    part_in.at[step - 1, span],
+                    send_part.at[step - 1, b],
+                    recv_part.at[step - 1, b],
+                    peer(step),
+                ).start()
+
+    x_copy.wait()
+
+    @pl.loop(0, products)
+    def _(i):
+        kind, index = product(i)
+
+        @pl.when(i + RING - 1 < products)
+        def _():
+            load(i + RING - 1)
+
+        arrived(wbuf.at[i % RING], w_sem.at[i % RING])
+        raw_ref[kind % 3] = jnp.dot(
+            x_ref[...], wbuf[i % RING], preferred_element_type=F32
+        ).astype(BF16)
+
+        @pl.when(i == 0)
+        def _():
+            early_sends()
+
+        @pl.when(jnp.logical_and(kind >= 4, j > 0))
+        def _():
+            @pl.when(jnp.logical_and(kind == 4, index == 0))
+            def _():
+                rim_copy.wait_recv()
+
+            rim_raw[kind - 4] = (
+                jnp.dot(rim_x[...], wbuf[i % RING], preferred_element_type=F32)
+                .astype(BF16)
+                .astype(F32)
+            )
+
+        @pl.when(i == 2)
+        def _():
+            local_weights()
+            sibling_weights()
+
+        @pl.when(kind == 1)
+        def _():
+            for p in range(per):
+                kv_own[0, index * per + p] = rotate(
+                    raw_ref[1, :, p * VD : (p + 1) * VD]
+                ).astype(BF16)
+            send_kv_of(0, index)
+
+        @pl.when(kind == 2)
+        def _():
+            for p in range(per):
+                kv_own[1, index * per + p] = raw_ref[2, :, p * VD : (p + 1) * VD]
+            send_kv_of(1, index)
+
+        @pl.when(kind == 0)
+        def _():
+            for p in range(per):
+                q_own[index * per + p] = (
+                    rotate(raw_ref[0, :, p * VD : (p + 1) * VD]) * fold
+                ).astype(BF16)
+            send_q_of(index)
+
+        @pl.when(kind == 5)
+        def _():
+            convolve(index)
 
     lam_copy.wait()
-
-    side = j // half
+    conv_copy.start()
+    keys_sent(side * half)
+    conv_parts()
+    pass_weights()
+
     head_at = (j % half) // repeat
     rep_at = j % repeat
     owner_tp = y * 2 + side
     lam = lam_all[side, pl.ds(head_at, 1)]
     gain = gain_ref[...].astype(F32)
     block_lane = lax.broadcasted_iota(jnp.int32, (rows, VD), 1)
-
-    def forward(block):
-        here = kv_all.at[c, block]
-        arrived(here, recv_kv.at[block])
-        remote(here, here, send_fwd.at[block], recv_fwd.at[block], sibling).start()
 
     def attend(slot, kb, both, part, masked):
         k, v = kv_all[0, kb], kv_all[1, kb]
@@ -423,94 +548,56 @@
                 index, theirs = piece_of(k, core, rank * 2 + 1 - c)
                 arrived(theirs, recv_s.at[rank, index])
 
-    def fix_first_rows():
-        @pl.when(j > 0)
-        def _():
-            rim_copy.wait_recv()
-
-        taps = taps_ref[...].astype(F32)
-        before = jnp.where(j > 0, rim_in[...], 0.0)
-        gated, gate = first_g[...], first_b[...]
-        row = lax.broadcasted_iota(jnp.int32, gated.shape, 0)
-        one, two = before[7:8], before[6:7]
-        back_one = jnp.where(row == 0, one, pltpu.roll(gated, 1, 0))
-        back_two = jnp.where(row == 0, two, jnp.where(row == 1, one, pltpu.roll(gated, 2, 0)))
-        conv = taps[0:1] * back_two + taps[1:2] * back_one + taps[2:3] * gated
-        conv_chip[c, :HEAD_ROWS] = (gate * conv).astype(BF16)
-
-    conv_copy = remote(
-        conv_chip.at[c], conv_chip.at[c], small_send.at[2], small_recv.at[2], sibling
-    )
-
-    def conv_product(first, rank):
-        span = pl.ds(first, SPAN)
-        return jnp.dot(
-            conv_chip[0, span], wc_all[rank, 0], preferred_element_type=F32
-        ) + jnp.dot(conv_chip[1, span], wc_all[rank, 1], preferred_element_type=F32)
-
-    def conv_parts():
-        conv_copy.wait_recv()
-
-        @pl.loop(0, ranks)
-        def _(rank):
-            mine = wc_all.at[rank, c]
-            theirs = wc_all.at[rank, 1 - c]
-            arrived(mine, local_wc.at[rank])
-            arrived(theirs, recv_wc.at[rank])
-
-        @pl.loop(1, ranks)
-        def _(step):
-            @pl.loop(0, tok // SPAN)
-            def _(b):
-                first = pl.multiple_of(b * SPAN, SPAN)
-                part_out[step - 1, pl.ds(first, SPAN)] = conv_product(
-                    first, (y + step) % ranks
-                ).astype(BF16)
-
-            remote(
-                part_out.at[step - 1],
-                part_in.at[step - 1],
-                send_part.at[step - 1],
-                recv_part.at[step - 1],
-                peer(step),
-            ).start()
-
     @pl.loop(0, 3 * half)
     def _(step):
         phase = step // half
         turn = (step + j) % half
-        group = jnp.where(phase == 0, side, jnp.where(phase == 1, 1 - side, 1))
+        group = jnp.where(phase == 0, side, jnp.where(phase == 1, 1, 1 - side))
         block = group * half + turn
         base = group * half
         slot = jnp.where(group == 0, half, turn)
-
-        @pl.when(jnp.logical_and(step % half == 0, phase < 2))
-        def _():
+        enter = step % half == 0
+        other = (1 - side) * half
+
+        def keys_ready(first):
             @pl.loop(0, half)
             def _(b):
-                forward(base + b)
-
+                arrived(kv_all.at[1 - c, first + b], recv_fwd.at[first + b])
+
+        def queries_ready(first):
             @pl.loop(0, half)
             def _(b):
-                arrived(q_all.at[base + b], recv_q.at[base + b])
-                arrived(kv_all.at[1 - c, base + b], recv_fwd.at[base + b])
-
-        @pl.when(step == 1)
-        def _():
-            fix_first_rows()
-            conv_copy.start()
-
-        @pl.when(step == 2)
-        def _():
-            conv_parts()
-
-        @pl.when(step > 2 * half)
-        def _():
-            share(step - 2 * half - 1)
-
-        @pl.when(step > 2 * half + 1)
-        def _():
-            relay(step - 2 * half - 2)
+                arrived(q_all.at[first + b], recv_q.at[first + b])
+
+        @pl.when(jnp.logical_and(enter, phase == 0))
+        def _():
+            keys_ready(base)
+            queries_ready(base)
+
+        @pl.when(jnp.logical_and(enter, phase == 1 + side))
+        def _():
+            queries_ready(other)
+
+        @pl.when(jnp.logical_and(enter, phase == 2 - side))
+        def _():
+            keys_sent(other)
+            keys_ready(other)
+
+        @pl.when(jnp.logical_and(early, step == 2 * half))
+        def _():
+            @pl.loop(0, half)
+            def _(k):
+                share(k)
+
+        @pl.when(jnp.logical_and(early, step == 2 * half + 2))
+        def _():
+            @pl.loop(0, half)
+            def _(k):
+                relay(k)
+
+        @pl.when(jnp.logical_and(jnp.logical_not(early), step > 2 * half + 1))
+        def _():
+            share(step - 2 * half - 2)
 
         q = q_all[block]
         zero = jnp.zeros_like(q)
@@ -519,21 +606,21 @@
         )
         part = part_of(block, rep_at, c)
 
-        @pl.when(phase < 2)
+        @pl.when(phase == jnp.where(group == 0, phase, 1 - side))
         def _():
             m_ref[slot] = jnp.full(m_ref.shape[1:], NEG_LARGE, F32)
             l_ref[slot] = jnp.zeros(l_ref.shape[1:], F32)
             acc_ref[slot] = jnp.zeros(acc_ref.shape[1:], F32)
 
-        @pl.loop(jnp.where(phase == 2, 0, base), jnp.where(phase == 2, half, block))
+        @pl.loop(jnp.where(phase == 1, 0, base), jnp.where(phase == 1, half, block))
         def _(kb):
             attend(slot, kb, both, part, False)
 
-        @pl.when(phase < 2)
+        @pl.when(phase != 1)
         def _():
             attend(slot, block, both, part, True)
 
-        @pl.when(jnp.logical_or(phase == 2, group == 0))
+        @pl.when(phase >= jnp.where(group == 0, 0, 2 - side))
         def _():
             first, second = (
                 acc_ref[slot, span] / jnp.sum(l_ref[slot, span], axis=1, keepdims=True)
@@ -551,12 +638,21 @@
                 jnp.logical_and(block == j, side == c),
             )
 
-    share(half - 1)
-    relay(half - 2)
+    @pl.when(jnp.logical_not(early))
+    def _():
+        @pl.loop(half - 2, half)
+        def _(k):
+            share(k)
+
+        @pl.loop(0, half - 1)
+        def _(k):
+            relay(k)
 
     @pl.loop(1, ranks)
     def _(step):
-        arrived(part_in.at[step - 1], recv_part.at[step - 1])
+        @pl.loop(0, tok // SPAN)
+        def _(b):
+            arrived(part_in.at[step - 1, pl.ds(0, SPAN)], recv_part.at[step - 1, b])
 
     @pl.loop(0, tok // SPAN)
     def _(b):
@@ -566,10 +662,18 @@
             value = value + part_in[step - 1, pl.ds(first, SPAN)].astype(F32)
         total_ref[pl.ds(first, SPAN)] = value
 
-    @pl.loop(0, tp)
-    def _(source):
-        for head in range(heads):
+    for head in range(heads):
+        for e in range(2):
+            source = y * 2 + e
             arrived(wa_rows(head, source), recv_wa.at[source, head])
+
+    @pl.loop(1, ranks)
+    def _(step):
+        for e in range(2):
+            source = (y + step) % ranks * 2 + e
+            for h in range(near):
+                head = near - first_near + h
+                arrived(wa_rows(head, source), recv_wa.at[source, head])
 
     def accumulate(k):
         gathered(k)
@@ -584,7 +688,7 @@
 
     @pl.loop(0, half)
     def _(k):
-        @pl.when(k == half - 1)
+        @pl.when(jnp.logical_and(jnp.logical_not(early), k == half - 1))
         def _():
             relay(half - 1)
 
@@ -619,8 +723,6 @@
     def _(step):
         stat_copy(step).start()
 
-    own_gain = out_gain_ref[:, pl.ds(pl.multiple_of(t * width, VD), width)].astype(F32)
-
     @pl.loop(1, tp)
     def _(step):
         source = (t + tp - step) % tp
@@ -635,12 +737,8 @@
             squares = squares + stats[source, 1:2, span]
         mean = sums / model
         scale = lax.rsqrt(squares / model - mean * mean + 1e-05)
-        mean_cols = jnp.broadcast_to(mean, (VD, SPAN)).T
-        scale_cols = jnp.broadcast_to(scale, (VD, SPAN)).T
-        for s in range(slabs):
-            cols = slice(s * VD, (s + 1) * VD)
-            value = (out_ref[span, cols].astype(F32) - mean_cols) * scale_cols
-            out_ref[span, cols] = (value * own_gain[:, cols]).astype(BF16)
+        stat_ref[0:1, span] = mean
+        stat_ref[1:2, span] = scale
 
 
     @pl.when(j + 1 < n)
@@ -674,8 +772,17 @@
     @pl.loop(1, tp)
     def _(step):
         stat_copy(step).wait_send()
-        for head in range(heads):
-            sent(wa_rows(head, t), send_wa.at[(t + step) % tp, head])
+
+    for head in range(heads):
+        sent(wa_rows(head, t), send_wa.at[y * 2 + 1 - c, head])
+
+    @pl.loop(1, ranks)
+    def _(step):
+        for e in range(2):
+            other = (y + step) % ranks * 2 + e
+            for h in range(near):
+                sent(wa_rows(h, t), send_wa.at[other, first_near + h])
+                sent(wa_rows(h, t), send_wf.at[other, h])
 
     @pl.loop(0, ranks)
     def _(rank):
@@ -683,7 +790,19 @@
 
     @pl.loop(1, ranks)
     def _(step):
-        sent(part_out.at[step - 1], send_part.at[step - 1])
+        @pl.loop(0, tok // SPAN)
+        def _(b):
+            sent(part_out.at[step - 1, pl.ds(0, SPAN)], send_part.at[step - 1, b])
+
+
+def scale_kernel(mix_ref, stat_ref, gain_ref, out_ref):
+    rows, width = mix_ref.shape
+    mean = jnp.broadcast_to(stat_ref[0:1], (VD, rows)).T
+    scale = jnp.broadcast_to(stat_ref[1:2], (VD, rows)).T
+    for s in range(width // VD):
+        cols = slice(s * VD, (s + 1) * VD)
+        value = (mix_ref[:, cols].astype(F32) - mean) * scale
+        out_ref[:, cols] = (value * gain_ref[:, cols]).astype(BF16)
 
 
 def per_device(
@@ -723,16 +842,21 @@
     vmem, hbm = pl.BlockSpec(memory_space=pltpu.VMEM), pl.BlockSpec(memory_space=pl.ANY)
     smem = pl.BlockSpec(memory_space=pltpu.SMEM)
     dma = pltpu.SemaphoreType.DMA
-    return pl.pallas_call(
+    mix, stat = pl.pallas_call(
         functools.partial(mixer_kernel, n, tp),
-        out_shape=jax.ShapeDtypeStruct((tok, width), BF16),
-        in_specs=[vmem] * 3 + [smem] + [vmem] * 2 + [hbm] * 9,
-        out_specs=vmem,
+        out_shape=(
+            jax.ShapeDtypeStruct((tok, width), BF16),
+            jax.ShapeDtypeStruct((8, tok), F32),
+        ),
+        in_specs=[hbm] + [vmem] * 2 + [smem] + [vmem] + [hbm] * 9,
+        out_specs=(vmem, vmem),
         scratch_shapes=[
             pltpu.VMEM((tok, model), BF16),
             pltpu.VMEM((tok, VD), F32),
             pltpu.VMEM((tok, VD), F32),
-            pltpu.VMEM((2, 3, model, TILE), BF16),
+            pltpu.VMEM((2, tok, VD), F32),
+            pltpu.VMEM((RING, model, TILE), BF16),
+            pltpu.VMEM((3, tok, TILE), BF16),
             pltpu.VMEM((heads, tok, VD), BF16),
             pltpu.VMEM((2, heads, tok, VD), BF16),
             pltpu.VMEM((n, rows, VD), BF16),
@@ -742,10 +866,8 @@
             pltpu.VMEM((half + 1, 2 * rows, VD), F32),
             pltpu.VMEM((half + 1, 2 * rows, VD), F32),
             pltpu.VMEM((2, lam_rows, VD), F32),
-            pltpu.VMEM((8, channels), F32),
-            pltpu.VMEM((8, channels), F32),
-            pltpu.VMEM((HEAD_ROWS, channels), F32),
-            pltpu.VMEM((HEAD_ROWS, channels), F32),
+            pltpu.VMEM((RIM, model), BF16),
+            pltpu.VMEM((2, RIM, TILE), F32),
             pltpu.VMEM((2, tok, channels), BF16),
             pltpu.VMEM((ranks, 2, channels, width), BF16),
             pltpu.VMEM((heads * tp * VD, width), BF16),
@@ -755,7 +877,8 @@
             pltpu.VMEM((tok, width), F32),
             pltpu.VMEM((tp, 8, tok), F32),
             dma,
-            dma((2, 3)),
+            dma,
+            dma((RING,)),
             dma((n,)),
             dma((n,)),
             dma((n,)),
@@ -768,11 +891,12 @@
             dma((3,)),
             dma((tp, heads)),
             dma((tp, heads)),
+            dma((tp, heads)),
             dma((ranks,)),
             dma((ranks,)),
             dma((ranks,)),
-            dma((ranks,)),
-            dma((ranks,)),
+            dma((ranks, tok // SPAN)),
+            dma((ranks, tok // SPAN)),
             dma((ranks, n)),
             dma((ranks, n)),
             dma((ranks, n)),
@@ -795,7 +919,6 @@
         conv_taps,
         lambdas,
         head_gain[None],
-        out_gain[None],
         hidden_states,
         w_query,
         w_key,
@@ -806,6 +929,23 @@
         w_out_conv,
         w_out_attn,
     )
+    own_gain = lax.dynamic_slice_in_dim(out_gain, lax.axis_index("tp") * width, width, 0)
+    grid = tok // SPAN
+    return pl.pallas_call(
+        scale_kernel,
+        grid=(grid,),
+        out_shape=jax.ShapeDtypeStruct((tok, width), BF16),
+        in_specs=[
+            pl.BlockSpec((SPAN, width), lambda i: (i, 0)),
+            pl.BlockSpec((8, SPAN), lambda i: (0, i)),
+            pl.BlockSpec((1, width), lambda i: (0, 0)),
+        ],
+        out_specs=pl.BlockSpec((SPAN, width), lambda i: (i, 0)),
+        cost_estimate=pl.CostEstimate(
+            flops=4 * tok * width, bytes_accessed=4 * tok * width, transcendentals=0
+        ),
+        name="scale",
+    )(mix, stat, own_gain.astype(F32)[None, :])
 
 
 def solution(mesh):

time: 141 us -> 126 us (0.89)
  the two profiles are of different devices: /device:TPU:23 before, /device:TPU:0 now
where the time goes in v1:
time: 126 us; the launch traced here: 125 us
  Pallas kernels  124 us (98%)
  other arithmetic  1.27 us (1%)
    pallas_call x1, Pallas kernels, per_device(): pl.pallas_call(functools.partial(mixer_kernel, n, tp), out_shape=(jax.Sha...  120 us
    pallas_call x1, Pallas kernels, per_device(): pl.pallas_call(scale_kernel, grid=(grid,), out_shape=jax.ShapeDtypeStruct...  3.77 us

profile of v1, /device:TPU:0, one launch (start us, length us, event | category | flops | bytes accessed | tf_op | source)
XLA Modules:
  0.0 125.4 jit_solution(16879051612679561918)
XLA Ops:
  0.0 1.3 %dynamic-slice_convert_fusion = f32[1024]{0:T(1024)} fusion(bf16[4096]{0:T(1024)(128)(2,1)} %param.27, s32[]{:T(128)S(6)} %select_n.3), kind=kLoop, calls=%fused_computation | loop fusion | flops 1024 | bytes 6148 | tf_op jit(solution)/shard_map/broadcast_in_dim | solution.py:948
  1.3 120.4 %mixer.1 = (bf16[768,1024]{1,0:T(8,128)(2,1)}, f32[8,768]{1,0:T(8,128)}) custom-call(f32[2,768,128]{2,1,0:T(8,128)} %constant.14.clone.turn_ref, f32[2,8,128]{2,1,0:T(8,128)} %constant.15.clone.base_ref, bf16[3,512]{1,0:T(4,128)(2,1)} %taps_ref.1, f32[4]{0:T(128)} %lam_ref.1, bf16[1,128]{1,0:T(2,128)(2,1)} %bitcast.3, bf16[768,4096]{1,0:T(8,128)(2,1)} %x_hbm.1, ...), custom_call_target="tpu_custom_call" | custom-call | flops 28991029248 | bytes 31457280 | tf_op jit(solution)/shard_map/mixer/pallas_call | solution.py:845
  121.6 3.8 %scale.1 = bf16[768,1024]{1,0:T(8,128)(2,1)} custom-call(bf16[768,1024]{1,0:T(8,128)(2,1)} %get-tuple-element.7.mix_ref, f32[8,768]{1,0:T(8,128)} %get-tuple-element.8.stat_ref, f32[1,1024]{1,0:T(1,128)} %bitcast.2), custom_call_target="tpu_custom_call" | custom-call | flops 3145728 | bytes 3145728 | tf_op jit(solution)/shard_map/scale/pallas_call | solution.py:934

commit v2 on v1

--- a/solution.py
+++ b/solution.py
@@ -64,6 +64,7 @@
     part_in,
     attn_all,
     total_ref,
+    mix_ref,
     stats,
     x_sem,
     turn_sem,
@@ -92,6 +93,7 @@
     recv_s,
     send_stat,
     recv_stat,
+    mix_sem,
 ):
     j, t = lax.axis_index("sp"), lax.axis_index("tp")
     c, y = t % 2, t // 2
@@ -132,14 +134,17 @@
     side = j // half
     early = c == side
     shift = jnp.where(jnp.logical_and(side == 1, c == 0), 0, 1)
-    lead = jnp.where(early, 0, 3 * ((tiles + 1) // 2))
+    lead = jnp.where(early, 0, tiles)
 
     def product(i):
         is_conv = jnp.logical_or(i < lead, i >= lead + 3 * pairs)
         r = jnp.where(i < lead, i, i - 3 * pairs)
         q = i - lead
-        kind = jnp.where(is_conv, 3 + r % 3, (q // pairs + shift) % 3)
-        index = jnp.where(is_conv, r // 3, (q % pairs + j) % pairs)
+        gate = r < tiles
+        conv_kind = jnp.where(gate, 3, 4 + (r - tiles) % 2)
+        conv_index = jnp.where(gate, r, (r - tiles) // 2)
+        kind = jnp.where(is_conv, conv_kind, (q // pairs + shift) % 3)
+        index = jnp.where(is_conv, conv_index, (q % pairs + j) % pairs)
         return kind, index
 
     def load(i):
@@ -197,8 +202,12 @@
     )
     lam_copy = remote(lam_all.at[c], lam_all.at[c], small_send.at[0], small_recv.at[0], sibling)
 
+    def place(head, source):
+        order = source % 2 * ranks + source // 2
+        return pl.multiple_of((head * tp + order) * VD, VD)
+
     def wa_rows(head, source):
-        return wa_all.at[pl.ds(pl.multiple_of((head * tp + source) * VD, VD), VD)]
+        return wa_all.at[pl.ds(place(head, source), VD)]
 
     def wa_block(head, target):
         return w_attn_ref.at[
@@ -360,7 +369,7 @@
         back_two = jnp.where(row == 0, two, jnp.where(row == 1, one, pltpu.roll(gated, 2, 0)))
         tap = taps_ref[:, cols].astype(F32)
         conv = tap[0:1] * back_two + tap[1:2] * back_one + tap[2:3] * gated
-        conv_chip[c, :, cols] = (raw_ref[0].astype(F32) * conv).astype(BF16)
+        conv_chip[c, :, cols] = (raw_ref[3 + g].astype(F32) * conv).astype(BF16)
 
 
     def forward(block):
@@ -419,7 +428,7 @@
             load(i + RING - 1)
 
         arrived(wbuf.at[i % RING], w_sem.at[i % RING])
-        raw_ref[kind % 3] = jnp.dot(
+        raw_ref[jnp.where(kind == 3, 3 + index, kind % 3)] = jnp.dot(
             x_ref[...], wbuf[i % RING], preferred_element_type=F32
         ).astype(BF16)
 
@@ -483,12 +492,24 @@
     gain = gain_ref[...].astype(F32)
     block_lane = lax.broadcasted_iota(jnp.int32, (rows, VD), 1)
 
-    def attend(slot, kb, both, part, masked):
-        k, v = kv_all[0, kb], kv_all[1, kb]
-        s = lax.dot_general(both, k, (((1,), (1,)), ((), ())), preferred_element_type=F32)
+    def scores(both, kb, part, masked):
+        s = lax.dot_general(
+            both, kv_all[0, kb], (((1,), (1,)), ((), ())), preferred_element_type=F32
+        )
         if masked:
             r = part * rows + lax.broadcasted_iota(jnp.int32, s.shape, 0) % rows
             s = jnp.where(lax.broadcasted_iota(jnp.int32, s.shape, 1) <= r, s, NEG_LARGE)
+        return s
+
+    def attend(slot, both, part, jobs):
+        ahead = scores(both, jobs[0][0], part, jobs[0][1])
+        for number, (kb, _) in enumerate(jobs):
+            s = ahead
+            if number + 1 < len(jobs):
+                ahead = scores(both, jobs[number + 1][0], part, jobs[number + 1][1])
+            weigh(slot, s, kv_all[1, kb])
+
+    def weigh(slot, s, v):
         slabs = [s[:, b * VD : (b + 1) * VD] for b in range(tok // VD)]
         old = m_ref[slot]
         top = functools.reduce(jnp.maximum, slabs)
@@ -509,7 +530,7 @@
     def piece(head, source, part):
         return attn_all.at[
             pl.ds(pl.multiple_of(part * rows, 16), rows),
-            pl.ds(pl.multiple_of((head * tp + source) * VD, VD), VD),
+            pl.ds(place(head, source), VD),
         ]
 
     def piece_of(k, core, source):
@@ -548,6 +569,21 @@
                 index, theirs = piece_of(k, core, rank * 2 + 1 - c)
                 arrived(theirs, recv_s.at[rank, index])
 
+    def own_product():
+        @pl.loop(1, ranks)
+        def _(step):
+            @pl.loop(0, tok // SPAN)
+            def _(b):
+                arrived(part_in.at[step - 1, pl.ds(0, SPAN)], recv_part.at[step - 1, b])
+
+        @pl.loop(0, tok // SPAN)
+        def _(b):
+            first = pl.multiple_of(b * SPAN, SPAN)
+            value = conv_product(first, y)
+            for step in range(1, ranks):
+                value = value + part_in[step - 1, pl.ds(first, SPAN)].astype(F32)
+            total_ref[pl.ds(first, SPAN)] = value
+
     @pl.loop(0, 3 * half)
     def _(step):
         phase = step // half
@@ -578,10 +614,17 @@
         def _():
             queries_ready(other)
 
+        @pl.when(step == jnp.where(side == 0, 2 * half - 1, half))
+        def _():
+            keys_sent(other)
+
         @pl.when(jnp.logical_and(enter, phase == 2 - side))
         def _():
-            keys_sent(other)
             keys_ready(other)
+
+        @pl.when(step == 2 * half + 2)
+        def _():
+            own_product()
 
         @pl.when(jnp.logical_and(early, step == 2 * half))
         def _():
@@ -612,13 +655,21 @@
             l_ref[slot] = jnp.zeros(l_ref.shape[1:], F32)
             acc_ref[slot] = jnp.zeros(acc_ref.shape[1:], F32)
 
-        @pl.loop(jnp.where(phase == 1, 0, base), jnp.where(phase == 1, half, block))
-        def _(kb):
-            attend(slot, kb, both, part, False)
-
-        @pl.when(phase != 1)
-        def _():
-            attend(slot, block, both, part, True)
+        low_kb = jnp.where(phase == 1, 0, base)
+        count = jnp.where(phase == 1, half, block - base)
+
+        @pl.loop(0, count // 2)
+        def _(p):
+            kb = low_kb + 2 * p
+            attend(slot, both, part, [(kb, False), (kb + 1, False)])
+
+        @pl.when(jnp.logical_and(phase != 1, count % 2 == 1))
+        def _():
+            attend(slot, both, part, [(block - 1, False), (block, True)])
+
+        @pl.when(jnp.logical_and(phase != 1, count % 2 == 0))
+        def _():
+            attend(slot, both, part, [(block, True)])
 
         @pl.when(phase >= jnp.where(group == 0, 0, 2 - side))
         def _():
@@ -638,30 +689,6 @@
                 jnp.logical_and(block == j, side == c),
             )
 
-    @pl.when(jnp.logical_not(early))
-    def _():
-        @pl.loop(half - 2, half)
-        def _(k):
-            share(k)
-
-        @pl.loop(0, half - 1)
-        def _(k):
-            relay(k)
-
-    @pl.loop(1, ranks)
-    def _(step):
-        @pl.loop(0, tok // SPAN)
-        def _(b):
-            arrived(part_in.at[step - 1, pl.ds(0, SPAN)], recv_part.at[step - 1, b])
-
-    @pl.loop(0, tok // SPAN)
-    def _(b):
-        first = pl.multiple_of(b * SPAN, SPAN)
-        value = conv_product(first, y)
-        for step in range(1, ranks):
-            value = value + part_in[step - 1, pl.ds(first, SPAN)].astype(F32)
-        total_ref[pl.ds(first, SPAN)] = value
-
     for head in range(heads):
         for e in range(2):
             source = y * 2 + e
@@ -675,11 +702,14 @@
                 head = near - first_near + h
                 arrived(wa_rows(head, source), recv_wa.at[source, head])
 
-    def accumulate(k):
-        gathered(k)
+    def accumulate(k, group):
+        @pl.when(c != group)
+        def _():
+            gathered(k)
+
         local = (j - k) % half
         head, rep = local // repeat, local % repeat
-        deep = pl.ds(pl.multiple_of(head * tp * VD, VD), tp * VD)
+        deep = pl.ds(place(head, group), ranks * VD)
         for core in range(2):
             span = pl.ds(pl.multiple_of(part_of(j, rep, core) * rows, 16), rows)
             total_ref[span] = total_ref[span] + jnp.dot(
@@ -688,19 +718,34 @@
 
     @pl.loop(0, half)
     def _(k):
-        @pl.when(jnp.logical_and(jnp.logical_not(early), k == half - 1))
-        def _():
-            relay(half - 1)
-
-        accumulate(k)
+        accumulate(k, side)
+
+    @pl.when(jnp.logical_not(early))
+    def _():
+        @pl.loop(half - 2, half)
+        def _(k):
+            share(k)
+
+        @pl.loop(0, half)
+        def _(k):
+            relay(k)
+
+    @pl.loop(0, half)
+    def _(k):
+        accumulate(k, 1 - side)
 
     slabs = width // VD
+
+    def mix_copy(b):
+        span = pl.ds(pl.multiple_of(b * SPAN, SPAN), SPAN)
+        return pltpu.make_async_copy(mix_ref.at[span], out_ref.at[span], mix_sem.at[b])
 
     @pl.loop(0, tok // SPAN)
     def _(b):
         span = pl.ds(pl.multiple_of(b * SPAN, SPAN), SPAN)
         mix = total_ref[span].astype(BF16)
-        out_ref[span] = mix
+        mix_ref[span] = mix
+        mix_copy(b).start()
         sums = jnp.zeros((SPAN, VD), F32)
         squares = jnp.zeros((SPAN, VD), F32)
         for s in range(slabs):
@@ -740,6 +785,10 @@
         stat_ref[0:1, span] = mean
         stat_ref[1:2, span] = scale
 
+
+    @pl.loop(0, tok // SPAN)
+    def _(b):
+        mix_copy(b).wait()
 
     @pl.when(j + 1 < n)
     def _():
@@ -849,14 +898,14 @@
             jax.ShapeDtypeStruct((8, tok), F32),
         ),
         in_specs=[hbm] + [vmem] * 2 + [smem] + [vmem] + [hbm] * 9,
-        out_specs=(vmem, vmem),
+        out_specs=(hbm, vmem),
         scratch_shapes=[
             pltpu.VMEM((tok, model), BF16),
             pltpu.VMEM((tok, VD), F32),
             pltpu.VMEM((tok, VD), F32),
             pltpu.VMEM((2, tok, VD), F32),
             pltpu.VMEM((RING, model, TILE), BF16),
-            pltpu.VMEM((3, tok, TILE), BF16),
+            pltpu.VMEM((3 + channels // TILE, tok, TILE), BF16),
             pltpu.VMEM((heads, tok, VD), BF16),
             pltpu.VMEM((2, heads, tok, VD), BF16),
             pltpu.VMEM((n, rows, VD), BF16),
@@ -875,6 +924,7 @@
             pltpu.VMEM((max(ranks - 1, 1), tok, width), BF16),
             pltpu.VMEM((tok, heads * tp * VD), BF16),
             pltpu.VMEM((tok, width), F32),
+            pltpu.VMEM((tok, width), BF16),
             pltpu.VMEM((tp, 8, tok), F32),
             dma,
             dma,
@@ -903,6 +953,7 @@
             dma((ranks, n)),
             dma((tp,)),
             dma((tp,)),
+            dma((tok // SPAN,)),
         ],
         compiler_params=pltpu.CompilerParams(
             vmem_limit_bytes=VMEM_LIMIT, collective_id=0, has_side_effects=True

time: 126 us -> 115 us (0.913)
  Pallas kernels: 124 us -> 114 us
    pallas_call x1, Pallas kernels: 120 us -> 110 us  [per_device(): pl.pallas_call(functools.partial(mixer_kernel, n, tp), out_shape=(jax.Sha...]
where the time goes in v2:
time: 115 us
  Pallas kernels  114 us (99%)
  other arithmetic  1.27 us (1%)
    pallas_call x1, Pallas kernels, per_device(): pl.pallas_call(functools.partial(mixer_kernel, n, tp), out_shape=(jax.Sha...  110 us
    pallas_call x1, Pallas kernels, per_device(): pl.pallas_call(scale_kernel, grid=(grid,), out_shape=jax.ShapeDtypeStruct...  3.77 us

profile of v2, /device:TPU:0, one launch (start us, length us, event | category | flops | bytes accessed | tf_op | source)
XLA Modules:
  0.0 115.0 jit_solution(8323414933299608399)
XLA Ops:
  0.0 1.3 %dynamic-slice_convert_fusion = f32[1024]{0:T(1024)} fusion(bf16[4096]{0:T(1024)(128)(2,1)} %param.27, s32[]{:T(128)S(6)} %select_n.3), kind=kLoop, calls=%fused_computation | loop fusion | flops 1024 | bytes 6148 | tf_op jit(solution)/shard_map/broadcast_in_dim | solution.py:999
  1.3 109.9 %mixer.1 = (bf16[768,1024]{1,0:T(8,128)(2,1)}, f32[8,768]{1,0:T(8,128)}) custom-call(f32[2,768,128]{2,1,0:T(8,128)} %constant.14.clone.turn_ref, f32[2,8,128]{2,1,0:T(8,128)} %constant.15.clone.base_ref, bf16[3,512]{1,0:T(4,128)(2,1)} %taps_ref.1, f32[4]{0:T(128)} %lam_ref.1, bf16[1,128]{1,0:T(2,128)(2,1)} %bitcast.3, bf16[768,4096]{1,0:T(8,128)(2,1)} %x_hbm.1, ...), custom_call_target="tpu_custom_call" | custom-call | flops 28991029248 | bytes 31457280 | tf_op jit(solution)/shard_map/mixer/pallas_call | solution.py:894
  111.2 3.8 %scale.1 = bf16[768,1024]{1,0:T(8,128)(2,1)} custom-call(bf16[768,1024]{1,0:T(8,128)(2,1)} %get-tuple-element.7.mix_ref, f32[8,768]{1,0:T(8,128)} %get-tuple-element.8.stat_ref, f32[1,1024]{1,0:T(1,128)} %bitcast.2), custom_call_target="tpu_custom_call" | custom-call | flops 3145728 | bytes 3145728 | tf_op jit(solution)/shard_map/scale/pallas_call | solution.py:985

commit v3 on v2

--- a/solution.py
+++ b/solution.py
@@ -25,10 +25,10 @@
     n,
     tp,
     turn_ref,
-    base_ref,
-    taps_ref,
+    base_hbm,
+    taps_hbm,
     lam_ref,
-    gain_ref,
+    gain_hbm,
     x_hbm,
     wq_ref,
     wk_ref,
@@ -66,8 +66,12 @@
     total_ref,
     mix_ref,
     stats,
+    base_ref,
+    taps_ref,
+    gain_ref,
     x_sem,
     turn_sem,
+    tiny_sem,
     w_sem,
     send_q,
     send_kv,
@@ -130,6 +134,14 @@
 
     turn_copy = pltpu.make_async_copy(turn_ref, tables, turn_sem)
     turn_copy.start()
+    tiny = [
+        pltpu.make_async_copy(src, dst, tiny_sem.at[i])
+        for i, (src, dst) in enumerate(
+            ((base_hbm, base_ref), (taps_hbm, taps_ref), (gain_hbm, gain_ref))
+        )
+    ]
+    for copy in tiny:
+        copy.start()
     products = 3 * (pairs + tiles)
     side = j // half
     early = c == side
@@ -181,6 +193,8 @@
                 device_id_type=MESH,
             )
 
+    for copy in tiny:
+        copy.wait()
     lane_row = lax.broadcasted_iota(jnp.int32, (1, VD), 1)
     cos_far, sin_far = base_ref[0, pl.ds(j, 1)], base_ref[1, pl.ds(j, 1)]
     turn_copy.wait()
@@ -218,8 +232,10 @@
     def wc_cols(rank, core):
         return w_conv_ref.at[:, pl.ds(pl.multiple_of((rank * 2 + core) * width, VD), width)]
 
-    near = heads // 2
-    first_near = (j % 2) * near
+    direct = heads // 2
+    passed = heads - direct
+    odd = j % 2
+    first_direct, first_passed, first_lacking = odd * passed, odd * direct, (1 - odd) * direct
 
     def local_weights():
         for head in range(heads):
@@ -244,8 +260,8 @@
         def _(step):
             for e in range(2):
                 target = (y + step) % ranks * 2 + e
-                for h in range(near):
-                    head = first_near + h
+                for h in range(direct):
+                    head = first_direct + h
                     remote(
                         wa_block(head, target),
                         wa_rows(head, t),
@@ -280,8 +296,8 @@
         def _(step):
             for e in range(2):
                 source = (y + step) % ranks * 2 + e
-                for h in range(near):
-                    head = first_near + h
+                for h in range(passed):
+                    head = first_passed + h
                     block = wa_rows(head, source)
                     arrived(block, recv_wa.at[source, head])
                     remote(
@@ -289,7 +305,7 @@
                         block,
                         send_wf.at[source, h],
                         recv_wa.at[source, head],
-                        (j + 1 - 2 * (j % 2), t),
+                        (j + 1 - 2 * odd, t),
                     ).start()
 
     def part_of(block, rep, core):
@@ -626,21 +642,21 @@
         def _():
             own_product()
 
-        @pl.when(jnp.logical_and(early, step == 2 * half))
+        @pl.when(jnp.logical_and(early, step == 2 * half + 1))
         def _():
             @pl.loop(0, half)
             def _(k):
                 share(k)
 
-        @pl.when(jnp.logical_and(early, step == 2 * half + 2))
+        @pl.when(jnp.logical_and(early, step == 2 * half + 3))
         def _():
             @pl.loop(0, half)
             def _(k):
                 relay(k)
 
-        @pl.when(jnp.logical_and(jnp.logical_not(early), step > 2 * half + 1))
-        def _():
-            share(step - 2 * half - 2)
+        @pl.when(jnp.logical_and(jnp.logical_not(early), step > 2 * half + 2))
+        def _():
+            share(step - 2 * half - 3)
 
         q = q_all[block]
         zero = jnp.zeros_like(q)
@@ -698,8 +714,11 @@
     def _(step):
         for e in range(2):
             source = (y + step) % ranks * 2 + e
-            for h in range(near):
-                head = near - first_near + h
+            for h in range(passed):
+                head = first_lacking + h
+                arrived(wa_rows(head, source), recv_wa.at[source, head])
+            for h in range(direct - passed):
+                head = passed + h
                 arrived(wa_rows(head, source), recv_wa.at[source, head])
 
     def accumulate(k, group):
@@ -722,7 +741,7 @@
 
     @pl.when(jnp.logical_not(early))
     def _():
-        @pl.loop(half - 2, half)
+        @pl.loop(half - 3, half)
         def _(k):
             share(k)
 
@@ -829,8 +848,9 @@
     def _(step):
         for e in range(2):
             other = (y + step) % ranks * 2 + e
-            for h in range(near):
-                sent(wa_rows(h, t), send_wa.at[other, first_near + h])
+            for h in range(direct):
+                sent(wa_rows(h, t), send_wa.at[other, first_direct + h])
+            for h in range(passed):
                 sent(wa_rows(h, t), send_wf.at[other, h])
 
     @pl.loop(0, ranks)
@@ -846,12 +866,17 @@
 
 def scale_kernel(mix_ref, stat_ref, gain_ref, out_ref):
     rows, width = mix_ref.shape
+    first = lax.axis_index("tp") * width
     mean = jnp.broadcast_to(stat_ref[0:1], (VD, rows)).T
     scale = jnp.broadcast_to(stat_ref[1:2], (VD, rows)).T
     for s in range(width // VD):
         cols = slice(s * VD, (s + 1) * VD)
         value = (mix_ref[:, cols].astype(F32) - mean) * scale
-        out_ref[:, cols] = (value * gain_ref[:, cols]).astype(BF16)
+        if s % 2 == 0:
+            at = pl.multiple_of(first + s * VD, 2 * VD)
+            gain = gain_ref[pl.ds(at, 2 * VD)].astype(F32).reshape(1, 2 * VD)
+        part = gain[:, s % 2 * VD : (s % 2 + 1) * VD]
+        out_ref[:, cols] = (value * part).astype(BF16)
 
 
 def per_device(
@@ -897,7 +922,7 @@
             jax.ShapeDtypeStruct((tok, width), BF16),
             jax.ShapeDtypeStruct((8, tok), F32),
         ),
-        in_specs=[hbm] + [vmem] * 2 + [smem] + [vmem] + [hbm] * 9,
+        in_specs=[hbm] * 3 + [smem] + [hbm] * 10,
         out_specs=(hbm, vmem),
         scratch_shapes=[
             pltpu.VMEM((tok, model), BF16),
@@ -926,8 +951,12 @@
             pltpu.VMEM((tok, width), F32),
             pltpu.VMEM((tok, width), BF16),
             pltpu.VMEM((tp, 8, tok), F32),
+            pltpu.VMEM((2, n, VD), F32),
+            pltpu.VMEM(conv_taps.shape, BF16),
+            pltpu.VMEM((1, VD), BF16),
             dma,
             dma,
+            dma((3,)),
             dma((RING,)),
             dma((n,)),
             dma((n,)),
@@ -980,7 +1009,6 @@
         w_out_conv,
         w_out_attn,
     )
-    own_gain = lax.dynamic_slice_in_dim(out_gain, lax.axis_index("tp") * width, width, 0)
     grid = tok // SPAN
     return pl.pallas_call(
         scale_kernel,
@@ -989,14 +1017,14 @@
         in_specs=[
             pl.BlockSpec((SPAN, width), lambda i: (i, 0)),
             pl.BlockSpec((8, SPAN), lambda i: (0, i)),
-            pl.BlockSpec((1, width), lambda i: (0, 0)),
+            pl.BlockSpec((model,), lambda i: (0,)),
         ],
         out_specs=pl.BlockSpec((SPAN, width), lambda i: (i, 0)),
         cost_estimate=pl.CostEstimate(
             flops=4 * tok * width, bytes_accessed=4 * tok * width, transcendentals=0
         ),
         name="scale",
-    )(mix, stat, own_gain.astype(F32)[None, :])
+    )(mix, stat, out_gain)
 
 
 def solution(mesh):

time: 115 us -> 111 us (0.965)
  Pallas kernels: 114 us -> 111 us
  other arithmetic: 1.27 us -> 0 us
    pallas_call x1, Pallas kernels: 110 us -> 107 us  [per_device(): pl.pallas_call(functools.partial(mixer_kernel, n, tp), out_shape=(jax.Sha...]
    broadcast_in_dim x1 -> x0, other arithmetic: 1.27 us -> none  [per_device(): own_gain.astype(F32)[None, :]]
where the time goes in v3:
time: 111 us
  Pallas kernels  111 us (100%)
    pallas_call x1, Pallas kernels, per_device(): pl.pallas_call(functools.partial(mixer_kernel, n, tp), out_shape=(jax.Sha...  107 us
    pallas_call x1, Pallas kernels, per_device(): pl.pallas_call(scale_kernel, grid=(grid,), out_shape=jax.ShapeDtypeStruct...  3.77 us

profile of v3, /device:TPU:0, one launch (start us, length us, event | category | flops | bytes accessed | tf_op | source)
XLA Modules:
  0.0 110.6 jit_solution(7150784515973654535)
XLA Ops:
  0.0 106.8 %mixer.1 = (bf16[768,1024]{1,0:T(8,128)(2,1)}, f32[8,768]{1,0:T(8,128)}) custom-call(f32[2,768,128]{2,1,0:T(8,128)} %constant.4.clone.turn_ref, f32[2,8,128]{2,1,0:T(8,128)} %constant.5.clone.base_hbm, bf16[3,512]{1,0:T(4,128)(2,1)} %taps_hbm.1, f32[4]{0:T(128)} %lam_ref.1, bf16[1,128]{1,0:T(2,128)(2,1)} %bitcast.1, bf16[768,4096]{1,0:T(8,128)(2,1)} %x_hbm.1, ...), custom_call_target="tpu_custom_call" | custom-call | flops 28991029248 | bytes 31457280 | tf_op jit(solution)/shard_map/mixer/pallas_call | solution.py:919
  106.8 3.8 %scale.1 = bf16[768,1024]{1,0:T(8,128)(2,1)} custom-call(bf16[768,1024]{1,0:T(8,128)(2,1)} %get-tuple-element.7.mix_ref, f32[8,768]{1,0:T(8,128)} %get-tuple-element.8.stat_ref, bf16[4096]{0:T(1024)(128)(2,1)} %gain_ref.1), custom_call_target="tpu_custom_call" | custom-call | flops 3145728 | bytes 3145728 | tf_op jit(solution)/shard_map/scale/pallas_call | solution.py:1013
